TPU v7x, 32 devices: a whole 2x2x4 slice. The times are simulated.
32 devices in a mesh: sp: 16 (over z, y, x), tp: 2 (over core).
Axes of the slice: x: 2, y: 2, z: 4, core: 2. Of those that a mesh axis runs over, the one named last changes fastest.
Arguments:
- residual_in: bfloat16 [6144, 2048], P(('sp', 'tp')), may hold values from -6 to 6
- conv_values: bfloat16 [6144, 1024], P('sp', 'tp'), may hold values from -60 to 60
- conv_gates: bfloat16 [6144, 1024], P('sp', 'tp'), may hold values from -8 to 8
- conv_kernel: float32 [31, 1024], P(None, 'tp'), may hold values from -1 to 1
- conv_bias: float32 [1024], P('tp'), may hold values from -3 to 3
- chan_gain: float32 [1024], P('tp'), may hold values from 0.1 to 1.9
- chan_shift: float32 [1024], P('tp'), may hold values from -3 to 3
- out_weight: bfloat16 [1024, 2048], replicated, may hold values from -0.1875 to 0.1875
- norm_gain: float32 [2048], replicated, may hold values from 0.1 to 1.9
- route_ids: int32 [6144, 2], P(('sp', 'tp')), may hold values from 0 to 15, all different within a row; in each aligned block of 192 rows (0 to 191, 192 to 383, ...) at most 48 rows name the same one
- route_weights: float32 [6144, 2], P(('sp', 'tp')), may hold values from 0.25 to 1.5
- expert_gate: bfloat16 [16, 2048, 2048], P('sp', None, 'tp'), may hold values from -0.125 to 0.125
- expert_up: bfloat16 [16, 2048, 2048], P('sp', None, 'tp'), may hold values from -0.125 to 0.125
- expert_down: bfloat16 [16, 2048, 2048], P('sp', 'tp'), may hold values from -0.125 to 0.125
Outputs:
- layer_out: bfloat16 [6144, 2048], P(('sp', 'tp'))
Inputs may be any that keep to these rules, and one draw needn't show every extreme that they name: `route_ids`: each row names 2 different experts. Among the rows of one device (aligned blocks of 192 rows) no expert is named by more than 48 rows, a bound that some block reaches.
All inputs are finite; a program needn't handle non-finite values.
Results may differ from a plain program's by a relative error of at most 0.014.
Values may be sent and summed in bfloat16 or wider, within the bound.
A program may use at most 128 MiB of HBM per device.

v0:
```python
import jax
import jax.numpy as jnp
from jax import lax
from jax.sharding import PartitionSpec as P


def from_behind(value, axis, steps):
    count = lax.axis_size(axis)
    first, last = (max(0, -steps), min(count, count - steps))
    return lax.ppermute(value, axis, [(source, source + steps) for source in range(first, last)])


def on_device(
    residual_in,
    conv_values,
    conv_gates,
    conv_kernel,
    conv_bias,
    chan_gain,
    chan_shift,
    out_weight,
    norm_gain,
    route_ids,
    route_weights,
    expert_gate,
    expert_up,
    expert_down,
):
    taps_count = conv_kernel.shape[0]
    tok_count, local_chan = conv_values.shape
    tp_count = lax.axis_size("tp")
    all_chan = local_chan * tp_count
    gated = (
        conv_values.astype(jnp.float32) * jax.nn.sigmoid(conv_gates.astype(jnp.float32))
    ).astype(jnp.bfloat16)
    earlier = from_behind(gated[tok_count - (taps_count - 1) :], "sp", 1)
    extended = jnp.concatenate([earlier, gated], 0).astype(jnp.float32)
    mixed = jnp.zeros((tok_count, local_chan), jnp.float32) + conv_bias[None, :]
    for tap_index in range(taps_count):
        mixed = (
            mixed + conv_kernel[tap_index][None, :] * extended[tap_index : tap_index + tok_count]
        )
    row_total = jnp.sum(mixed, 1)
    row_square = jnp.sum(mixed * mixed, 1)
    row_total, row_square = lax.psum((row_total, row_square), "tp")
    center = (row_total / all_chan)[:, None]
    spread = (row_square / all_chan)[:, None] - center * center
    normed = (mixed - center) * lax.rsqrt(spread + 1e-06) * chan_gain[None, :] + chan_shift[None, :]
    activated = jax.nn.silu(normed).astype(jnp.bfloat16)
    row_count = tok_count // tp_count
    regrouped = lax.all_to_all(activated, "tp", split_axis=0, concat_axis=1, tiled=True)
    projected = jnp.dot(regrouped, out_weight, preferred_element_type=jnp.float32)
    after_f = (residual_in.astype(jnp.float32) + projected).astype(jnp.bfloat16).astype(jnp.float32)
    normal_rows = (
        after_f
        * lax.rsqrt(jnp.mean(after_f * after_f, 1, keepdims=True) + 1e-06)
        * norm_gain[None, :]
    ).astype(jnp.bfloat16)
    model_width = normal_rows.shape[1]
    experts_all = expert_gate.shape[0] * lax.axis_size("sp")
    choose_count = route_ids.shape[1]
    slot_cap = max(2, (2 * choose_count * row_count + experts_all - 1) // experts_all)
    onehot = (
        route_ids.reshape(-1)[:, None] == jnp.arange(experts_all, dtype=jnp.int32)[None, :]
    ).astype(jnp.int32)
    before = jnp.cumsum(onehot, 0) - onehot
    ranking = jnp.sum(before * onehot, 1).reshape(row_count, choose_count)
    slot_ids = route_ids * slot_cap + ranking
    positions = lax.broadcasted_iota(jnp.int32, (experts_all * slot_cap, 1, 1), 0)
    dispatch = jnp.any(positions == slot_ids[None, :, :], axis=2).astype(jnp.bfloat16)
    sendable = jnp.dot(dispatch, normal_rows, preferred_element_type=jnp.float32).astype(
        jnp.bfloat16
    )
    sendable = sendable.reshape(experts_all, slot_cap, model_width)
    both_rows = lax.all_gather(
        lax.all_to_all(sendable, "sp", split_axis=0, concat_axis=0, tiled=True),
        "tp",
        axis=0,
        tiled=True,
    )
    leading, slot_width, widths = both_rows.shape
    flat_rows = both_rows.reshape(leading * slot_width, widths)
    gate = jnp.dot(flat_rows, expert_gate[0], preferred_element_type=jnp.float32)
    upper = jnp.dot(flat_rows, expert_up[0], preferred_element_type=jnp.float32)
    hidden = (jax.nn.silu(gate) * upper).astype(jnp.bfloat16)
    summed = lax.psum_scatter(
        jnp.dot(hidden, expert_down[0], preferred_element_type=jnp.float32)
        .reshape(leading, slot_width, widths)
        .astype(jnp.bfloat16),
        "tp",
        scatter_dimension=0,
        tiled=True,
    )
    results = lax.all_to_all(summed, "sp", split_axis=0, concat_axis=0, tiled=True)
    flat_out = results.reshape(experts_all * slot_cap, model_width)
    picked = (
        jnp.take(flat_out, slot_ids.reshape(-1), axis=0)
        .reshape(row_count, choose_count, model_width)
        .astype(jnp.float32)
    )
    combined = after_f + jnp.sum(route_weights[:, :, None] * picked, 1)
    return combined.astype(jnp.bfloat16)


def solution(mesh):
    placed = (
        P(("sp", "tp"), None),
        P("sp", "tp"),
        P("sp", "tp"),
        P(None, "tp"),
        P("tp"),
        P("tp"),
        P("tp"),
        P(),
        P(),
        P(("sp", "tp"), None),
        P(("sp", "tp"), None),
        P("sp", None, "tp"),
        P("sp", None, "tp"),
        P("sp", "tp", None),
    )
    return jax.shard_map(
        on_device, mesh=mesh, in_specs=placed, out_specs=P(("sp", "tp"), None), check_vma=False
    )
```

profile of v0, /device:TPU:14, one launch (start us, length us, event | category | flops | bytes accessed | tf_op | source)
XLA Modules:
  0.0 266.2 jit_solution(6359469079230641675)
XLA Ops:
  6.5 1.3 multiply_convert_fusion.4
  7.9 3.4 %collective-permute-start = (bf16[30,512]{1,0:T(8,128)(2,1)S(1)}, bf16[30,512]{1,0:T(8,128)(2,1)S(1)}, u32[]{:S(2)}, u32[]{:S(2)}) collective-permute-start(bf16[30,512]{1,0:T(8,128)(2,1)S(1)} %slice.262), channel_id=1, source_target_pairs={{0,2},{2,4},{4,6},{6,8},{8,10},{10,12},{12,14},{14,16},{16,18},{18... | collective-permute-start | bytes 92168 | tf_op jit(solution)/shard_map/ppermute | solution.py:10
  11.3 1.2 fusion.47
  12.5 1.0 fusion.48
  13.5 0.8 copy.42
  14.6 0.9 reduce-window.6
  15.5 0.2 slice_reduce_fusion
  15.8 0.1 reshape.98
  16.1 0.7 compare_and_fusion
  16.8 0.2 fusion.6
  17.1 3.8 %fusion.45 = (f32[384]{0:T(512)S(1)}, f32[384]{0:T(512)S(1)}, f32[384,512]{1,0:T(8,128)S(1)}) fusion(f32[414,512]{1,0:T(8,128)S(1)} %maximum_convert_fusion, f32[512]{0:T(512)S(1)} %bitcast.110, f32[512]{0:T(512)S(1)} %bitcast.111, f32[512]{0:T(512)S(1)} %bitcast.82, f32[512]{0:T(512)S(1)} %bitcast.83, f32[512]{0:T(512)S(1)} %bitcast.84, ...), kind=kLoop, calls=%fused_computation.104 | loop fusion | flops 12778752 | bytes 25234432 | tf_op jit(solution)/shard_map/reduce_sum | solution.py:43
  20.9 2.6 all-reduce
  23.6 0.4 multiply_convert_fusion.3
  23.9 4.0 %all_to_all.29 = bf16[2,192,512]{2,1,0:T(8,128)(2,1)S(1)} all-to-all(bf16[2,192,512]{2,1,0:T(8,128)(2,1)S(1)} %bitcast.79), channel_id=1, replica_groups=mesh['sp'=16,'tp'=2] {'tp'}, dimensions={0} | all-to-all | bytes 786432 | tf_op jit(solution)/shard_map/all_to_all | solution.py:51
  28.0 3.3 %multiply_reduce_fusion.1 = (f32[192]{0:T(256)S(1)}, f32[192,2048]{1,0:T(8,128)S(1)}) fusion(bf16[192,1024]{1,0:T(8,128)(2,1)S(1)} %bitcast.77, bf16[1024,2048]{1,0:T(8,128)(2,1)} %param.21, bf16[192,2048]{1,0:T(8,128)(2,1)S(1)} %copy-done.2), kind=kOutput, calls=%fused_computation.15 | convolution fusion | flops 807665472 | bytes 6947584 | tf_op jit(solution)/shard_map/dot_general | solution.py:52
  31.4 1.2 copy-done
  32.6 1.1 convolution_convert_fusion.1
  33.7 75.6 %all_to_all.30 = bf16[16,48,2048]{2,1,0:T(8,128)(2,1)} all-to-all(bf16[16,48,2048]{2,1,0:T(8,128)(2,1)S(1)} %bitcast.76), channel_id=1, replica_groups=mesh['sp'=16,'tp'=2] {'sp'}, dimensions={0} | all-to-all | bytes 6291456 | tf_op jit(solution)/shard_map/all_to_all | solution.py:76
  109.3 0.2 reduce-scatter.2.cloned.1.call-start
  109.5 16.9 %all-gather.2.cloned.1.call-done = bf16[32,48,2048]{2,1,0:T(8,128)(2,1)} async-done(((bf16[16,48,2048]{2,1,0:T(8,128)(2,1)}), bf16[32,48,2048]{2,1,0:T(8,128)(2,1)}) %all-gather.2.cloned.1.call-update) | async-done | bytes 6291472 | tf_op jit(solution)/shard_map/all_gather | solution.py:75
  126.4 10.1 %fusion.2 = f32[1536,1024]{1,0:T(8,128)S(1)} fusion(bf16[1536,2048]{1,0:T(8,128)(2,1)} %bitcast.112, bf16[1,2048,1024]{2,1,0:T(8,128)(2,1)} %param.25), kind=kOutput, calls=%fused_computation.5 | convolution fusion | flops 6442450944 | bytes 16777216 | tf_op jit(solution)/shard_map/dot_general | solution.py:83
  136.6 7.4 %multiply_convert_fusion = bf16[1536,1024]{1,0:T(8,128)(2,1)S(1)} fusion(f32[1536,1024]{1,0:T(8,128)S(1)} %fusion.2, bf16[1536,2048]{1,0:T(8,128)(2,1)S(1)} %bitcast.113, bf16[1,2048,1024]{2,1,0:T(8,128)(2,1)S(1)} %copy-done.9), kind=kOutput, calls=%fused_computation.1 | convolution fusion | flops 6451888128 | bytes 19922944 | tf_op jit(solution)/shard_map/dot_general | solution.py:84
  144.1 8.8 %convolution_convert_fusion = bf16[32,48,2048]{2,1,0:T(8,128)(2,1)} fusion(bf16[32,48,1024]{2,1,0:T(8,128)(2,1)S(1)} %bitcast.114, bf16[1,1024,2048]{2,1,0:T(8,128)(2,1)S(1)} %copy-done.10), kind=kOutput, calls=%fused_computation.2 | convolution fusion | flops 6445596672 | bytes 13631488 | tf_op jit(solution)/shard_map/dot_general | solution.py:87
  152.9 16.2 %reduce-scatter.2.cloned.1.call-done = bf16[16,48,2048]{2,1,0:T(8,128)(2,1)} async-done(((bf16[32,48,2048]{2,1,0:T(8,128)(2,1)}), bf16[16,48,2048]{2,1,0:T(8,128)(2,1)}) %reduce-scatter.2.cloned.1.call-update) | async-done | bytes 3145744 | tf_op jit(solution)/shard_map/reduce_scatter | solution.py:86
  169.1 7.0 %all-to-all-start.2 = ((bf16[16,48,2048]{2,1,0:T(8,128)(2,1)}), bf16[16,48,2048]{2,1,0:T(8,128)(2,1)S(1)}, u32[]{:S(2)}, u32[]{:S(2)}) async-start(bf16[16,48,2048]{2,1,0:T(8,128)(2,1)} %reduce-scatter.2.cloned.1.call-done), calls=%async_computation.3 | async-start | bytes 6291456 | tf_op jit(solution)/shard_map/all_to_all | solution.py:94
  176.2 0.1 reshape.102
  176.3 0.2 copy.46
  176.6 69.5 %all-to-all-done.2 = bf16[16,48,2048]{2,1,0:T(8,128)(2,1)S(1)} async-done(((bf16[16,48,2048]{2,1,0:T(8,128)(2,1)}), bf16[16,48,2048]{2,1,0:T(8,128)(2,1)S(1)}, u32[]{:S(2)}, u32[]{:S(2)}) %all-to-all-start.2) | async-done | bytes 3145760 | tf_op jit(solution)/shard_map/all_to_all | solution.py:94
  246.1 3.1 %gather_fusion = bf16[384,2048]{1,0:T(8,128)(2,1)} fusion(bf16[768,2048]{1,0:T(8,128)(2,1)S(1)} %bitcast.75, s32[1024]{0:T(1024)S(1)} %pad_clamp_fusion), kind=kCustom, calls=%fused_computation | custom fusion | bytes 3147264 | tf_op jit(solution)/shard_map/jit(_take)/gather | solution.py:97
  249.2 2.9 %gather.7 = bf16[192,2,2048]{2,1,0:T(2,128)(2,1)S(1)} reshape(bf16[384,2048]{1,0:T(8,128)(2,1)} %gather_fusion) | data formatting | bytes 3145728 | tf_op jit(solution)/shard_map/jit(_take)/gather | solution.py:97
  252.1 6.1 %multiply_reduce_fusion = f32[192,2048]{1,0:T(8,128)S(1)} fusion(bf16[192,2,2048]{2,1,0:T(2,128)(2,1)S(1)} %gather.7, pred[192,2]{1,0:T(8,128)(4,1)S(1)} %copy.46, f32[192,2]{1,0:T(8,128)S(1)} %copy.41), kind=kLoop, calls=%fused_computation.8 | loop fusion | flops 2752512 | bytes 3147648 | tf_op jit(solution)/shard_map/reduce_sum | solution.py:101
  258.3 1.1 add_convert_fusion
  (40 shorter events, 1.0 us)
Async XLA Ops:
  6.5 10.5 %copy-start.7 = (f32[512]{0:T(512)S(1)}, f32[512]{0:T(512)}, u32[]{:S(2)}) copy-start(f32[512]{0:T(512)} %param.18) | copy-start | bytes 6148
  6.5 119.9 %all-gather.2.cloned.1.call-start = ((), (), s32[]{:S(2)}) async-start(), calls=%async_computation.4 | async-start | bytes 9437184 | tf_op jit(solution)/shard_map/all_gather | solution.py:75
  7.9 9.0 %collective-permute-start = (bf16[30,512]{1,0:T(8,128)(2,1)S(1)}, bf16[30,512]{1,0:T(8,128)(2,1)S(1)}, u32[]{:S(2)}, u32[]{:S(2)}) collective-permute-start(bf16[30,512]{1,0:T(8,128)(2,1)S(1)} %slice.262), channel_id=1, source_target_pairs={{0,2},{2,4},{4,6},{6,8},{8,10},{10,12},{12,14},{14,16},{16,18},{18... | collective-permute-start | bytes 92168 | tf_op jit(solution)/shard_map/ppermute | solution.py:10
  17.1 6.5 %copy-start.4 = (f32[512]{0:T(512)S(1)}, f32[512]{0:T(512)}, u32[]{:S(2)}) copy-start(f32[512]{0:T(512)} %param.20) | copy-start | bytes 6148
  17.1 6.5 %copy-start.5 = (f32[512]{0:T(512)S(1)}, f32[512]{0:T(512)}, u32[]{:S(2)}) copy-start(f32[512]{0:T(512)} %param.19) | copy-start | bytes 6148
  20.9 7.1 %copy-start.2 = (bf16[192,2048]{1,0:T(8,128)(2,1)S(1)}, bf16[192,2048]{1,0:T(8,128)(2,1)}, u32[]{:S(2)}) copy-start(bf16[192,2048]{1,0:T(8,128)(2,1)} %param.14) | copy-start | bytes 2359300
  28.0 4.5 %copy-start.3 = (f32[2048]{0:T(1024)S(1)}, f32[2048]{0:T(1024)}, u32[]{:S(2)}) copy-start(f32[2048]{0:T(1024)} %param.22) | copy-start | bytes 24580
  31.4 1.2 copy-start
  109.3 59.8 %reduce-scatter.2.cloned.1.call-start = ((), (), s32[]{:S(2)}) async-start(), calls=%async_computation.5 | async-start | bytes 9437184 | tf_op jit(solution)/shard_map/reduce_scatter | solution.py:86
  126.4 10.1 %copy-start.8 = (bf16[32,48,2048]{2,1,0:T(8,128)(2,1)S(1)}, bf16[32,48,2048]{2,1,0:T(8,128)(2,1)}, u32[]{:S(2)}) copy-start(bf16[32,48,2048]{2,1,0:T(8,128)(2,1)} %all-gather.2.cloned.1.call-done) | copy-start | bytes 18874372
  126.4 10.1 %copy-start.9 = (bf16[1,2048,1024]{2,1,0:T(8,128)(2,1)S(1)}, bf16[1,2048,1024]{2,1,0:T(8,128)(2,1)}, u32[]{:S(2)}) copy-start(bf16[1,2048,1024]{2,1,0:T(8,128)(2,1)} %param.26) | copy-start | bytes 12582916
  136.6 7.5 %copy-start.10 = (bf16[1,1024,2048]{2,1,0:T(8,128)(2,1)S(1)}, bf16[1,1024,2048]{2,1,0:T(8,128)(2,1)}, u32[]{:S(2)}) copy-start(bf16[1,1024,2048]{2,1,0:T(8,128)(2,1)} %param.27) | copy-start | bytes 12582916
  152.9 23.6 %copy-start.6 = (f32[192,2]{0,1:T(2,128)S(1)}, f32[192,2]{0,1:T(2,128)}, u32[]{:S(2)}) copy-start(f32[192,2]{0,1:T(2,128)} %param.24) | copy-start | bytes 4612
  169.1 77.0 %all-to-all-start.2 = ((bf16[16,48,2048]{2,1,0:T(8,128)(2,1)}), bf16[16,48,2048]{2,1,0:T(8,128)(2,1)S(1)}, u32[]{:S(2)}, u32[]{:S(2)}) async-start(bf16[16,48,2048]{2,1,0:T(8,128)(2,1)} %reduce-scatter.2.cloned.1.call-done), calls=%async_computation.3 | async-start | bytes 6291456 | tf_op jit(solution)/shard_map/all_to_all | solution.py:94
  249.2 9.0 %copy-start.1 = (f32[192,2048]{1,0:T(8,128)S(1)}, f32[192,2048]{1,0:T(8,128)}, u32[]{:S(2)}) copy-start(f32[192,2048]{1,0:T(8,128)} %copy-done) | copy-start | bytes 4718596
Sparse Core Ops, SparseCore 0:
  109.4 16.9 all-gather.1
  153.0 16.0 reduce-scatter.1
where the time goes:
time: 267 us; the launch traced here: 266 us
  waiting for transfers between devices  103 us (39%)
  blocking collectives  82.3 us (31%)
  matrix products  30.7 us (11%)
  other arithmetic  14.8 us (6%)
  between operations  13.7 us (5%)
  local copies, waits for them, and re-layouts  11.5 us (4%)
  starting transfers between devices  10.6 us (4%)
    all_to_all x1, blocking collectives, on_device(): lax.all_to_all(sendable, 'sp', split_axis=0, concat_axis=0, tiled=True)  75.6 us
    all_to_all x1, waiting for transfers between devices, on_device(): lax.all_to_all(summed, 'sp', split_axis=0, concat_axis=0, tiled=True)  69.5 us
    all_gather x1, waiting for transfers between devices, on_device(): lax.all_gather(lax.all_to_all(sendable, 'sp', split_axis=0, concat_axis=0...  16.9 us
    reduce_scatter x1, waiting for transfers between devices, on_device(): lax.psum_scatter(jnp.dot(hidden, expert_down[0], preferred_element_type=j...  16.2 us
    dot_general x1, matrix products, on_device(): jnp.dot(flat_rows, expert_gate[0], preferred_element_type=jnp.float32)  10.1 us
    dot_general x1, matrix products, on_device(): jnp.dot(hidden, expert_down[0], preferred_element_type=jnp.float32)  8.76 us
    dot_general x1, matrix products, on_device(): upper = jnp.dot(flat_rows, expert_up[0], preferred_element_type=jnp.float32)  7.44 us
    all_to_all x1, starting transfers between devices, on_device(): lax.all_to_all(summed, 'sp', split_axis=0, concat_axis=0, tiled=True)  6.96 us
  transfers between devices with their start and end apart: 4, of which 3 were waited for; matrix products, arithmetic and copies ran while one was open for 2% of the time, Pallas kernels for 0%

commit v1 on v0

--- a/solution.py
+++ b/solution.py
@@ -2,6 +2,22 @@
 import jax.numpy as jnp
 from jax import lax
 from jax.sharding import PartitionSpec as P
+
+
+def swapped_with_each(value, axis, split, join):
+    ways, here = (lax.axis_size(axis), lax.axis_index(axis))
+    width = value.shape[split] // ways
+    shape = list(value.shape)
+    shape[split] = width
+    height = shape[join]
+    shape[join] = height * ways
+    full = jnp.zeros(shape, value.dtype)
+    for mask in range(ways):
+        part = lax.dynamic_slice_in_dim(value, (here ^ mask) * width, width, axis=split)
+        if mask:
+            part = lax.ppermute(part, axis, [(d, d ^ mask) for d in range(ways)])
+        full = lax.dynamic_update_slice_in_dim(full, part, (here ^ mask) * height, axis=join)
+    return full
 
 
 def from_behind(value, axis, steps):
@@ -72,12 +88,7 @@
         jnp.bfloat16
     )
     sendable = sendable.reshape(experts_all, slot_cap, model_width)
-    both_rows = lax.all_gather(
-        lax.all_to_all(sendable, "sp", split_axis=0, concat_axis=0, tiled=True),
-        "tp",
-        axis=0,
-        tiled=True,
-    )
+    both_rows = lax.all_gather(swapped_with_each(sendable, "sp", 0, 0), "tp", axis=0, tiled=True)
     leading, slot_width, widths = both_rows.shape
     flat_rows = both_rows.reshape(leading * slot_width, widths)
     gate = jnp.dot(flat_rows, expert_gate[0], preferred_element_type=jnp.float32)

time: 267 us -> 279 us (1.045)
  blocking collectives: 82.3 us -> 6.65 us
  waiting for transfers between devices: 103 us -> 164 us
  starting transfers between devices: 10.6 us -> 35.5 us
    all_to_all x1 -> x0, blocking collectives: 75.6 us -> none  [on_device(): lax.all_to_all(sendable, 'sp', split_axis=0, concat_axis=0, tiled=True)]
    ppermute x0 -> x15, waiting for transfers between devices: none -> 60.4 us  [swapped_with_each(): part = lax.ppermute(part, axis, [(d, d ^ mask) for d in range(ways)])]
    ppermute x0 -> x15, starting transfers between devices: none -> 24.9 us  [swapped_with_each(): part = lax.ppermute(part, axis, [(d, d ^ mask) for d in range(ways)])]
  transfers between devices with their start and end apart: 4 -> 19, of which waited for: 3 -> 15; matrix products, arithmetic and copies ran while one was open for 2% -> 2% of each run, Pallas kernels for 0% -> 0%
where the time goes in v1:
time: 279 us; the launch traced here: 278 us
  waiting for transfers between devices  164 us (59%)
  starting transfers between devices  35.5 us (13%)
  matrix products  30.4 us (11%)
  other arithmetic  14.7 us (5%)
  between operations  13.9 us (5%)
  local copies, waits for them, and re-layouts  13.2 us (5%)
  blocking collectives  6.65 us (2%)
    all_to_all x1, waiting for transfers between devices, on_device(): lax.all_to_all(summed, 'sp', split_axis=0, concat_axis=0, tiled=True)  69.5 us
    ppermute x15, waiting for transfers between devices, swapped_with_each(): part = lax.ppermute(part, axis, [(d, d ^ mask) for d in range(ways)])  60.4 us
    ppermute x15, starting transfers between devices, swapped_with_each(): part = lax.ppermute(part, axis, [(d, d ^ mask) for d in range(ways)])  24.9 us
    all_gather x1, waiting for transfers between devices, on_device(): lax.all_gather(swapped_with_each(sendable, 'sp', 0, 0), 'tp', axis=0, til...  17.6 us
    reduce_scatter x1, waiting for transfers between devices, on_device(): lax.psum_scatter(jnp.dot(hidden, expert_down[0], preferred_element_type=j...  16.2 us
    dot_general x1, matrix products, on_device(): jnp.dot(flat_rows, expert_gate[0], preferred_element_type=jnp.float32)  10.1 us
    dot_general x1, matrix products, on_device(): jnp.dot(hidden, expert_down[0], preferred_element_type=jnp.float32)  8.63 us
    dot_general x1, matrix products, on_device(): upper = jnp.dot(flat_rows, expert_up[0], preferred_element_type=jnp.float32)  7.24 us
  transfers between devices with their start and end apart: 19, of which 15 were waited for; matrix products, arithmetic and copies ran while one was open for 2% of the time, Pallas kernels for 0%

profile of v1, /device:TPU:14, one launch (start us, length us, event | category | flops | bytes accessed | tf_op | source)
XLA Modules:
  0.0 278.1 jit_solution(14589423367348707010)
XLA Ops:
  7.9 3.4 %collective-permute-start = (bf16[30,512]{1,0:T(8,128)(2,1)S(1)}, bf16[30,512]{1,0:T(8,128)(2,1)S(1)}, u32[]{:S(2)}, u32[]{:S(2)}) collective-permute-start(bf16[30,512]{1,0:T(8,128)(2,1)S(1)} %slice.262), channel_id=1, source_target_pairs={{0,2},{2,4},{4,6},{6,8},{8,10},{10,12},{12,14},{14,16},{16,18},{18... | collective-permute-start | bytes 92168 | tf_op jit(solution)/shard_map/ppermute | solution.py:26
  17.2 3.8 %fusion.48 = (f32[384]{0:T(512)S(1)}, f32[384]{0:T(512)S(1)}, f32[384,512]{1,0:T(8,128)S(1)}) fusion(f32[414,512]{1,0:T(8,128)S(1)} %maximum_convert_fusion, f32[512]{0:T(512)S(1)} %bitcast.112, f32[512]{0:T(512)S(1)} %bitcast.113, f32[512]{0:T(512)S(1)} %bitcast.84, f32[512]{0:T(512)S(1)} %bitcast.85, f32[512]{0:T(512)S(1)} %bitcast.86, ...), kind=kLoop, calls=%fused_computation.136 | loop fusion | flops 12778752 | bytes 25234432 | tf_op jit(solution)/shard_map/reduce_sum | solution.py:59
  21.0 2.6 all-reduce
  24.0 4.0 %all_to_all.24 = bf16[2,192,512]{2,1,0:T(8,128)(2,1)S(1)} all-to-all(bf16[2,192,512]{2,1,0:T(8,128)(2,1)S(1)} %bitcast.81), channel_id=1, replica_groups=mesh['sp'=16,'tp'=2] {'tp'}, dimensions={0} | all-to-all | bytes 786432 | tf_op jit(solution)/shard_map/all_to_all | solution.py:67
  28.1 3.3 %multiply_reduce_fusion.1 = (f32[192]{0:T(256)S(1)}, f32[192,2048]{1,0:T(8,128)S(1)}) fusion(bf16[192,1024]{1,0:T(8,128)(2,1)S(1)} %bitcast.79, bf16[1024,2048]{1,0:T(8,128)(2,1)} %param.21, bf16[192,2048]{1,0:T(8,128)(2,1)S(1)} %copy-done.3), kind=kOutput, calls=%fused_computation.16 | convolution fusion | flops 807665472 | bytes 6947584 | tf_op jit(solution)/shard_map/dot_general | solution.py:68
  34.6 2.5 collective-permute-start.3
  39.0 2.3 collective-permute-done.1
  42.0 2.3 collective-permute-start.7
  44.3 4.4 %collective-permute-done.3 = bf16[1,48,2048]{2,1,0:T(8,128)(2,1)S(1)} collective-permute-done((bf16[1,48,2048]{2,1,0:T(8,128)(2,1)S(1)}, bf16[1,48,2048]{2,1,0:T(8,128)(2,1)S(1)}, u32[]{:S(2)}, u32[]{:S(2)}) %collective-permute-start.3) | collective-permute-done | bytes 196640 | tf_op jit(solution)/shard_map/ppermute | solution.py:18
  48.8 2.6 collective-permute-start.8
  51.5 4.2 %collective-permute-start.10 = (bf16[1,48,2048]{2,1,0:T(8,128)(2,1)S(1)}, bf16[1,48,2048]{2,1,0:T(8,128)(2,1)S(1)}, u32[]{:S(2)}, u32[]{:S(2)}) collective-permute-start(bf16[1,48,2048]{2,1,0:T(8,128)(2,1)S(1)} %get-tuple-element.17), channel_id=1, source_target_pairs={{0,20},{2,22},{4,16},{6,18},{8,28},{10,30},{12,24},{14,26},{16,4},... | collective-permute-start | bytes 589832 | tf_op jit(solution)/shard_map/ppermute | solution.py:18
  55.7 2.7 collective-permute-done.6
  58.4 4.7 %collective-permute-start.11 = (bf16[1,48,2048]{2,1,0:T(8,128)(2,1)S(1)}, bf16[1,48,2048]{2,1,0:T(8,128)(2,1)S(1)}, u32[]{:S(2)}, u32[]{:S(2)}) collective-permute-start(bf16[1,48,2048]{2,1,0:T(8,128)(2,1)S(1)} %get-tuple-element.16), channel_id=1, source_target_pairs={{0,22},{2,20},{4,18},{6,16},{8,30},{10,28},{12,26},{14,24},{16,6},... | collective-permute-start | bytes 589832 | tf_op jit(solution)/shard_map/ppermute | solution.py:18
  63.8 16.1 %collective-permute-done.8 = bf16[1,48,2048]{2,1,0:T(8,128)(2,1)S(1)} collective-permute-done((bf16[1,48,2048]{2,1,0:T(8,128)(2,1)S(1)}, bf16[1,48,2048]{2,1,0:T(8,128)(2,1)S(1)}, u32[]{:S(2)}, u32[]{:S(2)}) %collective-permute-start.8) | collective-permute-done | bytes 196640 | tf_op jit(solution)/shard_map/ppermute | solution.py:18
  79.9 4.2 %collective-permute-done.9 = bf16[1,48,2048]{2,1,0:T(8,128)(2,1)S(1)} collective-permute-done((bf16[1,48,2048]{2,1,0:T(8,128)(2,1)S(1)}, bf16[1,48,2048]{2,1,0:T(8,128)(2,1)S(1)}, u32[]{:S(2)}, u32[]{:S(2)}) %collective-permute-start.9) | collective-permute-done | bytes 196640 | tf_op jit(solution)/shard_map/ppermute | solution.py:18
  84.0 4.5 %collective-permute-start.14 = (bf16[1,48,2048]{2,1,0:T(8,128)(2,1)S(1)}, bf16[1,48,2048]{2,1,0:T(8,128)(2,1)S(1)}, u32[]{:S(2)}, u32[]{:S(2)}) collective-permute-start(bf16[1,48,2048]{2,1,0:T(8,128)(2,1)S(1)} %get-tuple-element.13), channel_id=1, source_target_pairs={{0,28},{2,30},{4,24},{6,26},{8,20},{10,22},{12,16},{14,18},{16,12}... | collective-permute-start | bytes 589832 | tf_op jit(solution)/shard_map/ppermute | solution.py:18
  88.6 6.1 %collective-permute-done.10 = bf16[1,48,2048]{2,1,0:T(8,128)(2,1)S(1)} collective-permute-done((bf16[1,48,2048]{2,1,0:T(8,128)(2,1)S(1)}, bf16[1,48,2048]{2,1,0:T(8,128)(2,1)S(1)}, u32[]{:S(2)}, u32[]{:S(2)}) %collective-permute-start.10) | collective-permute-done | bytes 196640 | tf_op jit(solution)/shard_map/ppermute | solution.py:18
  94.7 6.2 %collective-permute-done.11 = bf16[1,48,2048]{2,1,0:T(8,128)(2,1)S(1)} collective-permute-done((bf16[1,48,2048]{2,1,0:T(8,128)(2,1)S(1)}, bf16[1,48,2048]{2,1,0:T(8,128)(2,1)S(1)}, u32[]{:S(2)}, u32[]{:S(2)}) %collective-permute-start.11) | collective-permute-done | bytes 196640 | tf_op jit(solution)/shard_map/ppermute | solution.py:18
  100.9 6.3 %collective-permute-done.12 = bf16[1,48,2048]{2,1,0:T(8,128)(2,1)S(1)} collective-permute-done((bf16[1,48,2048]{2,1,0:T(8,128)(2,1)S(1)}, bf16[1,48,2048]{2,1,0:T(8,128)(2,1)S(1)}, u32[]{:S(2)}, u32[]{:S(2)}) %collective-permute-start.12) | collective-permute-done | bytes 196640 | tf_op jit(solution)/shard_map/ppermute | solution.py:18
  107.2 4.2 %collective-permute-done.13 = bf16[1,48,2048]{2,1,0:T(8,128)(2,1)S(1)} collective-permute-done((bf16[1,48,2048]{2,1,0:T(8,128)(2,1)S(1)}, bf16[1,48,2048]{2,1,0:T(8,128)(2,1)S(1)}, u32[]{:S(2)}, u32[]{:S(2)}) %collective-permute-start.13) | collective-permute-done | bytes 196640 | tf_op jit(solution)/shard_map/ppermute | solution.py:18
  111.5 6.2 %collective-permute-done.14 = bf16[1,48,2048]{2,1,0:T(8,128)(2,1)S(1)} collective-permute-done((bf16[1,48,2048]{2,1,0:T(8,128)(2,1)S(1)}, bf16[1,48,2048]{2,1,0:T(8,128)(2,1)S(1)}, u32[]{:S(2)}, u32[]{:S(2)}) %collective-permute-start.14) | collective-permute-done | bytes 196640 | tf_op jit(solution)/shard_map/ppermute | solution.py:18
  119.1 1.7 copy-done.2
  121.0 17.6 %all-gather.2.cloned.1.call-done = bf16[32,48,2048]{2,1,0:T(8,128)(2,1)} async-done(((bf16[16,48,2048]{2,1,0:T(8,128)(2,1)}), bf16[32,48,2048]{2,1,0:T(8,128)(2,1)}) %all-gather.2.cloned.1.call-update) | async-done | bytes 6291472 | tf_op jit(solution)/shard_map/all_gather | solution.py:91
  138.7 10.1 %fusion.5 = f32[1536,1024]{1,0:T(8,128)S(1)} fusion(bf16[1536,2048]{1,0:T(8,128)(2,1)} %bitcast.114, bf16[1,2048,1024]{2,1,0:T(8,128)(2,1)} %param.25), kind=kOutput, calls=%fused_computation.6 | convolution fusion | flops 6442450944 | bytes 16777216 | tf_op jit(solution)/shard_map/dot_general | solution.py:94
  148.8 7.2 %multiply_convert_fusion = bf16[1536,1024]{1,0:T(8,128)(2,1)S(1)} fusion(f32[1536,1024]{1,0:T(8,128)S(1)} %fusion.5, bf16[1536,2048]{1,0:T(8,128)(2,1)S(1)} %bitcast.115, bf16[1,2048,1024]{2,1,0:T(8,128)(2,1)S(1)} %copy-done.10), kind=kOutput, calls=%fused_computation.1 | convolution fusion | flops 6451888128 | bytes 19922944 | tf_op jit(solution)/shard_map/dot_general | solution.py:95
  156.1 8.6 %convolution_convert_fusion = bf16[32,48,2048]{2,1,0:T(8,128)(2,1)} fusion(bf16[32,48,1024]{2,1,0:T(8,128)(2,1)S(1)} %bitcast.116, bf16[1,1024,2048]{2,1,0:T(8,128)(2,1)S(1)} %copy-done.11), kind=kOutput, calls=%fused_computation.2 | convolution fusion | flops 6445596672 | bytes 13631488 | tf_op jit(solution)/shard_map/dot_general | solution.py:98
  164.7 16.2 %reduce-scatter.2.cloned.1.call-done = bf16[16,48,2048]{2,1,0:T(8,128)(2,1)} async-done(((bf16[32,48,2048]{2,1,0:T(8,128)(2,1)}), bf16[16,48,2048]{2,1,0:T(8,128)(2,1)}) %reduce-scatter.2.cloned.1.call-update) | async-done | bytes 3145744 | tf_op jit(solution)/shard_map/reduce_scatter | solution.py:97
  181.0 7.0 %all-to-all-start.1 = ((bf16[16,48,2048]{2,1,0:T(8,128)(2,1)}), bf16[16,48,2048]{2,1,0:T(8,128)(2,1)S(1)}, u32[]{:S(2)}, u32[]{:S(2)}) async-start(bf16[16,48,2048]{2,1,0:T(8,128)(2,1)} %reduce-scatter.2.cloned.1.call-done), calls=%async_computation.2 | async-start | bytes 6291456 | tf_op jit(solution)/shard_map/all_to_all | solution.py:105
  188.5 69.5 %all-to-all-done.1 = bf16[16,48,2048]{2,1,0:T(8,128)(2,1)S(1)} async-done(((bf16[16,48,2048]{2,1,0:T(8,128)(2,1)}), bf16[16,48,2048]{2,1,0:T(8,128)(2,1)S(1)}, u32[]{:S(2)}, u32[]{:S(2)}) %all-to-all-start.1) | async-done | bytes 3145760 | tf_op jit(solution)/shard_map/all_to_all | solution.py:105
  258.0 3.1 %gather_fusion = bf16[384,2048]{1,0:T(8,128)(2,1)} fusion(bf16[768,2048]{1,0:T(8,128)(2,1)S(1)} %bitcast.77, s32[1024]{0:T(1024)S(1)} %pad_clamp_fusion), kind=kCustom, calls=%fused_computation | custom fusion | bytes 3147264 | tf_op jit(solution)/shard_map/jit(_take)/gather | solution.py:108
  261.1 2.9 %gather.7 = bf16[192,2,2048]{2,1,0:T(2,128)(2,1)S(1)} reshape(bf16[384,2048]{1,0:T(8,128)(2,1)} %gather_fusion) | data formatting | bytes 3145728 | tf_op jit(solution)/shard_map/jit(_take)/gather | solution.py:108
  264.0 6.1 %multiply_reduce_fusion = f32[192,2048]{1,0:T(8,128)S(1)} fusion(bf16[192,2,2048]{2,1,0:T(2,128)(2,1)S(1)} %gather.7, pred[192,2]{1,0:T(8,128)(4,1)S(1)} %copy.46, f32[192,2]{1,0:T(8,128)S(1)} %copy.41), kind=kLoop, calls=%fused_computation.9 | loop fusion | flops 2752512 | bytes 3147648 | tf_op jit(solution)/shard_map/reduce_sum | solution.py:112
  (88 shorter events, 17.5 us)
Async XLA Ops:
  6.5 10.6 %copy-start.8 = (f32[512]{0:T(512)S(1)}, f32[512]{0:T(512)}, u32[]{:S(2)}) copy-start(f32[512]{0:T(512)} %param.18) | copy-start | bytes 6148
  6.5 132.1 %all-gather.2.cloned.1.call-start = ((), (), s32[]{:S(2)}) async-start(), calls=%async_computation.3 | async-start | bytes 9437184 | tf_op jit(solution)/shard_map/all_gather | solution.py:91
  7.9 9.1 %collective-permute-start = (bf16[30,512]{1,0:T(8,128)(2,1)S(1)}, bf16[30,512]{1,0:T(8,128)(2,1)S(1)}, u32[]{:S(2)}, u32[]{:S(2)}) collective-permute-start(bf16[30,512]{1,0:T(8,128)(2,1)S(1)} %slice.262), channel_id=1, source_target_pairs={{0,2},{2,4},{4,6},{6,8},{8,10},{10,12},{12,14},{14,16},{16,18},{18... | collective-permute-start | bytes 92168 | tf_op jit(solution)/shard_map/ppermute | solution.py:26
  17.2 6.5 %copy-start.5 = (f32[512]{0:T(512)S(1)}, f32[512]{0:T(512)}, u32[]{:S(2)}) copy-start(f32[512]{0:T(512)} %param.20) | copy-start | bytes 6148
  17.2 6.5 %copy-start.6 = (f32[512]{0:T(512)S(1)}, f32[512]{0:T(512)}, u32[]{:S(2)}) copy-start(f32[512]{0:T(512)} %param.19) | copy-start | bytes 6148
  21.0 7.1 %copy-start.3 = (bf16[192,2048]{1,0:T(8,128)(2,1)S(1)}, bf16[192,2048]{1,0:T(8,128)(2,1)}, u32[]{:S(2)}) copy-start(bf16[192,2048]{1,0:T(8,128)(2,1)} %param.14) | copy-start | bytes 2359300
  28.1 3.4 %copy-start.4 = (f32[2048]{0:T(1024)S(1)}, f32[2048]{0:T(1024)}, u32[]{:S(2)}) copy-start(f32[2048]{0:T(1024)} %param.22) | copy-start | bytes 24580
  31.5 1.5 copy-start
  33.5 7.8 %collective-permute-start.1 = (bf16[1,48,2048]{2,1,0:T(8,128)(2,1)S(1)}, bf16[1,48,2048]{2,1,0:T(8,128)(2,1)S(1)}, u32[]{:S(2)}, u32[]{:S(2)}) collective-permute-start(bf16[1,48,2048]{2,1,0:T(8,128)(2,1)S(1)} %get-tuple-element.26), channel_id=1, source_target_pairs={{0,2},{2,0},{4,6},{6,4},{8,10},{10,8},{12,14},{14,12},{16,18},{18,... | collective-permute-start | bytes 589832 | tf_op jit(solution)/shard_map/ppermute | solution.py:18
  34.1 7.9 %collective-permute-start.2 = (bf16[1,48,2048]{2,1,0:T(8,128)(2,1)S(1)}, bf16[1,48,2048]{2,1,0:T(8,128)(2,1)S(1)}, u32[]{:S(2)}, u32[]{:S(2)}) collective-permute-start(bf16[1,48,2048]{2,1,0:T(8,128)(2,1)S(1)} %get-tuple-element.25), channel_id=1, source_target_pairs={{0,4},{2,6},{4,0},{6,2},{8,12},{10,14},{12,8},{14,10},{16,20},{18,... | collective-permute-start | bytes 589832 | tf_op jit(solution)/shard_map/ppermute | solution.py:18
  34.6 14.2 %collective-permute-start.3 = (bf16[1,48,2048]{2,1,0:T(8,128)(2,1)S(1)}, bf16[1,48,2048]{2,1,0:T(8,128)(2,1)S(1)}, u32[]{:S(2)}, u32[]{:S(2)}) collective-permute-start(bf16[1,48,2048]{2,1,0:T(8,128)(2,1)S(1)} %get-tuple-element.24), channel_id=1, source_target_pairs={{0,6},{2,4},{4,2},{6,0},{8,14},{10,12},{12,10},{14,8},{16,22},{18,... | collective-permute-start | bytes 589832 | tf_op jit(solution)/shard_map/ppermute | solution.py:18
  37.0 14.3 %collective-permute-start.4 = (bf16[1,48,2048]{2,1,0:T(8,128)(2,1)S(1)}, bf16[1,48,2048]{2,1,0:T(8,128)(2,1)S(1)}, u32[]{:S(2)}, u32[]{:S(2)}) collective-permute-start(bf16[1,48,2048]{2,1,0:T(8,128)(2,1)S(1)} %get-tuple-element.23), channel_id=1, source_target_pairs={{0,8},{2,10},{4,12},{6,14},{8,0},{10,2},{12,4},{14,6},{16,24},{18,... | collective-permute-start | bytes 589832 | tf_op jit(solution)/shard_map/ppermute | solution.py:18
  37.5 14.0 %collective-permute-start.5 = (bf16[1,48,2048]{2,1,0:T(8,128)(2,1)S(1)}, bf16[1,48,2048]{2,1,0:T(8,128)(2,1)S(1)}, u32[]{:S(2)}, u32[]{:S(2)}) collective-permute-start(bf16[1,48,2048]{2,1,0:T(8,128)(2,1)S(1)} %get-tuple-element.22), channel_id=1, source_target_pairs={{0,10},{2,8},{4,14},{6,12},{8,2},{10,0},{12,6},{14,4},{16,26},{18,... | collective-permute-start | bytes 589832 | tf_op jit(solution)/shard_map/ppermute | solution.py:18
  41.3 17.0 %collective-permute-start.6 = (bf16[1,48,2048]{2,1,0:T(8,128)(2,1)S(1)}, bf16[1,48,2048]{2,1,0:T(8,128)(2,1)S(1)}, u32[]{:S(2)}, u32[]{:S(2)}) collective-permute-start(bf16[1,48,2048]{2,1,0:T(8,128)(2,1)S(1)} %get-tuple-element.21), channel_id=1, source_target_pairs={{0,12},{2,14},{4,8},{6,10},{8,4},{10,6},{12,0},{14,2},{16,28},{18,... | collective-permute-start | bytes 589832 | tf_op jit(solution)/shard_map/ppermute | solution.py:18
  42.0 21.1 %collective-permute-start.7 = (bf16[1,48,2048]{2,1,0:T(8,128)(2,1)S(1)}, bf16[1,48,2048]{2,1,0:T(8,128)(2,1)S(1)}, u32[]{:S(2)}, u32[]{:S(2)}) collective-permute-start(bf16[1,48,2048]{2,1,0:T(8,128)(2,1)S(1)} %get-tuple-element.20), channel_id=1, source_target_pairs={{0,14},{2,12},{4,10},{6,8},{8,6},{10,4},{12,2},{14,0},{16,30},{18,... | collective-permute-start | bytes 589832 | tf_op jit(solution)/shard_map/ppermute | solution.py:18
  48.8 31.1 %collective-permute-start.8 = (bf16[1,48,2048]{2,1,0:T(8,128)(2,1)S(1)}, bf16[1,48,2048]{2,1,0:T(8,128)(2,1)S(1)}, u32[]{:S(2)}, u32[]{:S(2)}) collective-permute-start(bf16[1,48,2048]{2,1,0:T(8,128)(2,1)S(1)} %get-tuple-element.19), channel_id=1, source_target_pairs={{0,16},{2,18},{4,20},{6,22},{8,24},{10,26},{12,28},{14,30},{16,0},... | collective-permute-start | bytes 589832 | tf_op jit(solution)/shard_map/ppermute | solution.py:18
  51.4 32.6 %collective-permute-start.9 = (bf16[1,48,2048]{2,1,0:T(8,128)(2,1)S(1)}, bf16[1,48,2048]{2,1,0:T(8,128)(2,1)S(1)}, u32[]{:S(2)}, u32[]{:S(2)}) collective-permute-start(bf16[1,48,2048]{2,1,0:T(8,128)(2,1)S(1)} %get-tuple-element.18), channel_id=1, source_target_pairs={{0,18},{2,16},{4,22},{6,20},{8,26},{10,24},{12,30},{14,28},{16,2},... | collective-permute-start | bytes 589832 | tf_op jit(solution)/shard_map/ppermute | solution.py:18
  51.5 43.2 %collective-permute-start.10 = (bf16[1,48,2048]{2,1,0:T(8,128)(2,1)S(1)}, bf16[1,48,2048]{2,1,0:T(8,128)(2,1)S(1)}, u32[]{:S(2)}, u32[]{:S(2)}) collective-permute-start(bf16[1,48,2048]{2,1,0:T(8,128)(2,1)S(1)} %get-tuple-element.17), channel_id=1, source_target_pairs={{0,20},{2,22},{4,16},{6,18},{8,28},{10,30},{12,24},{14,26},{16,4},... | collective-permute-start | bytes 589832 | tf_op jit(solution)/shard_map/ppermute | solution.py:18
  58.4 42.5 %collective-permute-start.11 = (bf16[1,48,2048]{2,1,0:T(8,128)(2,1)S(1)}, bf16[1,48,2048]{2,1,0:T(8,128)(2,1)S(1)}, u32[]{:S(2)}, u32[]{:S(2)}) collective-permute-start(bf16[1,48,2048]{2,1,0:T(8,128)(2,1)S(1)} %get-tuple-element.16), channel_id=1, source_target_pairs={{0,22},{2,20},{4,18},{6,16},{8,30},{10,28},{12,26},{14,24},{16,6},... | collective-permute-start | bytes 589832 | tf_op jit(solution)/shard_map/ppermute | solution.py:18
  63.1 44.1 %collective-permute-start.12 = (bf16[1,48,2048]{2,1,0:T(8,128)(2,1)S(1)}, bf16[1,48,2048]{2,1,0:T(8,128)(2,1)S(1)}, u32[]{:S(2)}, u32[]{:S(2)}) collective-permute-start(bf16[1,48,2048]{2,1,0:T(8,128)(2,1)S(1)} %get-tuple-element.15), channel_id=1, source_target_pairs={{0,24},{2,26},{4,28},{6,30},{8,16},{10,18},{12,20},{14,22},{16,8},... | collective-permute-start | bytes 589832 | tf_op jit(solution)/shard_map/ppermute | solution.py:18
  79.8 31.6 %collective-permute-start.13 = (bf16[1,48,2048]{2,1,0:T(8,128)(2,1)S(1)}, bf16[1,48,2048]{2,1,0:T(8,128)(2,1)S(1)}, u32[]{:S(2)}, u32[]{:S(2)}) collective-permute-start(bf16[1,48,2048]{2,1,0:T(8,128)(2,1)S(1)} %get-tuple-element.14), channel_id=1, source_target_pairs={{0,26},{2,24},{4,30},{6,28},{8,18},{10,16},{12,22},{14,20},{16,10}... | collective-permute-start | bytes 589832 | tf_op jit(solution)/shard_map/ppermute | solution.py:18
  84.0 33.6 %collective-permute-start.14 = (bf16[1,48,2048]{2,1,0:T(8,128)(2,1)S(1)}, bf16[1,48,2048]{2,1,0:T(8,128)(2,1)S(1)}, u32[]{:S(2)}, u32[]{:S(2)}) collective-permute-start(bf16[1,48,2048]{2,1,0:T(8,128)(2,1)S(1)} %get-tuple-element.13), channel_id=1, source_target_pairs={{0,28},{2,30},{4,24},{6,26},{8,20},{10,22},{12,16},{14,18},{16,12}... | collective-permute-start | bytes 589832 | tf_op jit(solution)/shard_map/ppermute | solution.py:18
  94.7 24.4 %collective-permute-start.15 = (bf16[1,48,2048]{2,1,0:T(8,128)(2,1)S(1)}, bf16[1,48,2048]{2,1,0:T(8,128)(2,1)S(1)}, u32[]{:S(2)}, u32[]{:S(2)}) collective-permute-start(bf16[1,48,2048]{2,1,0:T(8,128)(2,1)S(1)} %get-tuple-element.12), channel_id=1, source_target_pairs={{0,30},{2,28},{4,26},{6,24},{8,22},{10,20},{12,18},{14,16},{16,14}... | collective-permute-start | bytes 589832 | tf_op jit(solution)/shard_map/ppermute | solution.py:18
  119.1 1.7 copy-start.2
  120.8 60.1 %reduce-scatter.2.cloned.1.call-start = ((), (), s32[]{:S(2)}) async-start(), calls=%async_computation.4 | async-start | bytes 9437184 | tf_op jit(solution)/shard_map/reduce_scatter | solution.py:97
  138.7 10.1 %copy-start.9 = (bf16[32,48,2048]{2,1,0:T(8,128)(2,1)S(1)}, bf16[32,48,2048]{2,1,0:T(8,128)(2,1)}, u32[]{:S(2)}) copy-start(bf16[32,48,2048]{2,1,0:T(8,128)(2,1)} %all-gather.2.cloned.1.call-done) | copy-start | bytes 18874372
  138.7 10.1 %copy-start.10 = (bf16[1,2048,1024]{2,1,0:T(8,128)(2,1)S(1)}, bf16[1,2048,1024]{2,1,0:T(8,128)(2,1)}, u32[]{:S(2)}) copy-start(bf16[1,2048,1024]{2,1,0:T(8,128)(2,1)} %param.26) | copy-start | bytes 12582916
  148.8 7.3 %copy-start.11 = (bf16[1,1024,2048]{2,1,0:T(8,128)(2,1)S(1)}, bf16[1,1024,2048]{2,1,0:T(8,128)(2,1)}, u32[]{:S(2)}) copy-start(bf16[1,1024,2048]{2,1,0:T(8,128)(2,1)} %param.27) | copy-start | bytes 12582916
  164.7 23.6 %copy-start.7 = (f32[192,2]{0,1:T(2,128)S(1)}, f32[192,2]{0,1:T(2,128)}, u32[]{:S(2)}) copy-start(f32[192,2]{0,1:T(2,128)} %param.24) | copy-start | bytes 4612
  181.0 77.0 %all-to-all-start.1 = ((bf16[16,48,2048]{2,1,0:T(8,128)(2,1)}), bf16[16,48,2048]{2,1,0:T(8,128)(2,1)S(1)}, u32[]{:S(2)}, u32[]{:S(2)}) async-start(bf16[16,48,2048]{2,1,0:T(8,128)(2,1)} %reduce-scatter.2.cloned.1.call-done), calls=%async_computation.2 | async-start | bytes 6291456 | tf_op jit(solution)/shard_map/all_to_all | solution.py:105
  261.1 9.0 %copy-start.1 = (f32[192,2048]{1,0:T(8,128)S(1)}, f32[192,2048]{1,0:T(8,128)}, u32[]{:S(2)}) copy-start(f32[192,2048]{1,0:T(8,128)} %copy-done) | copy-start | bytes 4718596
Sparse Core Ops, SparseCore 0:
  120.9 17.6 all-gather.1
  164.9 16.0 reduce-scatter.1
